TPU v7x, 512 devices: a whole 4x4x16 slice. The times are simulated.
512 devices in a mesh: fs: 128 (over z, x, core), tp: 4 (over y).
Axes of the slice: x: 4, y: 4, z: 16, core: 2. Of those that a mesh axis runs over, the one named last changes fastest.
Arguments:
- tokens: bfloat16 [768, 4096], P('tp'), may hold values from -6 to 6
- norm_gain: float32 [4096], P('fs'), may hold values from 0.1 to 1.9
- gate_trained: float32 [4096, 11264], P('fs', 'tp'), may hold values from -0.09375 to 0.09375
- up_trained: float32 [4096, 11264], P('fs', 'tp'), may hold values from -0.09375 to 0.09375
- down_trained: float32 [11264, 4096], P('fs', 'tp'), may hold values from -0.21875 to 0.21875
Outputs:
- gate_sampler: bfloat16 [4096, 11264], P(None, 'fs')
- up_sampler: bfloat16 [4096, 11264], P(None, 'fs')
- down_sampler: bfloat16 [11264, 4096], P('fs')
- mixed_out: bfloat16 [768, 4096], P('tp', 'fs')
All inputs are finite; a program needn't handle non-finite values.
Results may differ from a plain program's by a relative error of at most 0.0082.
Values may be sent and summed in bfloat16 or wider, within the bound.
A program may use at most 64 MiB of HBM per device.

v0:
```python
import jax
import jax.numpy as jnp
from jax import lax
from jax.sharding import Mesh
from jax.sharding import PartitionSpec as P

FS = ("fs_0", "fs_1", "fs_2")


def in_one_piece(arrays, axis, split_dim, concat_dim, along):
    ends, at = ([], 0)
    for a in arrays[:-1]:
        at += a.shape[along]
        ends.append(at)
    both = jnp.concatenate(arrays, axis=along)
    return tuple(
        jnp.split(
            lax.all_to_all(both, axis, split_axis=split_dim, concat_axis=concat_dim, tiled=True),
            ends,
            axis=along,
        )
    )


def in_one_piece_2(arrays, axis, dim, along):
    widths = [a.shape[along] for a in arrays]
    both = jnp.concatenate(arrays, axis=along)
    filled = lax.all_gather(both, axis, axis=dim, tiled=True)
    return tuple(jnp.split(filled, [sum(widths[:k]) for k in range(1, len(widths))], axis=along))


def in_blocks(array, dim, count):
    before, after = (array.shape[:dim], array.shape[dim + 1 :])
    return jnp.moveaxis(array.reshape(*before, count, -1, *after), dim, 0)


def sent_and_summed(array, axis, dim):
    count = lax.axis_size(axis)
    parts = lax.all_to_all(in_blocks(array, dim, count), axis, 0, 0, tiled=True)
    return jnp.sum(parts.astype(jnp.float32), axis=0)


def sum_by_axis(array, axes, dim):
    far, near = axes
    own = sent_and_summed(in_blocks(array, dim, lax.axis_size(far)), near, dim + 1)
    return jnp.sum(
        lax.all_to_all(own.astype(jnp.bfloat16), far, 0, 0, tiled=True).astype(jnp.float32), axis=0
    )


def per_device(tokens, norm_gain, gate_trained, up_trained, down_trained):
    gate_local = (norm_gain[:, None] * gate_trained).astype(jnp.bfloat16)
    up_local = (norm_gain[:, None] * up_trained).astype(jnp.bfloat16)
    down_local = down_trained.astype(jnp.bfloat16)
    tp_count = lax.axis_size("tp")
    fs_count = lax.axis_size(FS)
    rows_local = gate_local.shape[0]
    cols_local = gate_local.shape[1]
    model_width = rows_local * fs_count
    owned_count = cols_local * tp_count // fs_count
    piece_cols = owned_count // tp_count
    block_count = cols_local // owned_count

    def arrange(matrix):
        return matrix.reshape(rows_local, block_count, tp_count, piece_cols)

    gate_mixed, up_mixed = in_one_piece((arrange(gate_local), arrange(up_local)), "tp", 2, 2, 0)

    def regroup(matrix):
        return matrix.transpose(2, 1, 0, 3).reshape(fs_count, rows_local, piece_cols)

    gate_parts, up_parts = in_one_piece((regroup(gate_mixed), regroup(up_mixed)), FS, 0, 1, 2)
    gate_sampler, up_sampler, down_sampler = (
        *in_one_piece_2(
            (
                gate_parts.reshape(model_width, piece_cols),
                up_parts.reshape(model_width, piece_cols),
            ),
            "tp",
            1,
            0,
        ),
        lax.all_gather(down_local, "tp", axis=1, tiled=True),
    )
    as_float = tokens.astype(jnp.float32)
    normed = (
        as_float * lax.rsqrt(jnp.mean(as_float * as_float, axis=-1, keepdims=True) + 1e-06)
    ).astype(jnp.bfloat16)
    gate_act = jnp.dot(normed, gate_sampler, preferred_element_type=jnp.float32)
    up_act = jnp.dot(normed, up_sampler, preferred_element_type=jnp.float32)
    hidden = (jax.nn.silu(gate_act) * up_act).astype(jnp.bfloat16)
    partial_terms = jnp.dot(hidden, down_sampler, preferred_element_type=jnp.float32)
    mixed_out = sum_by_axis(
        partial_terms.astype(jnp.bfloat16), (("fs_0", "fs_1"), "fs_2"), 1
    ).astype(jnp.bfloat16)
    return (gate_sampler, up_sampler, down_sampler, mixed_out)


def solution(mesh):
    split = Mesh(mesh.devices.reshape(16, 4, 2, mesh.shape["tp"]), ("fs_0", "fs_1", "fs_2", "tp"))
    in_specs = (P("tp", None), P(FS), P(FS, "tp"), P(FS, "tp"), P(FS, "tp"))
    out_specs = (P(None, FS), P(None, FS), P(FS, None), P("tp", FS))
    return jax.shard_map(
        per_device, mesh=split, in_specs=in_specs, out_specs=out_specs, check_vma=False
    )
```

profile of v0, /device:TPU:1, one launch (start us, length us, event | category | flops | bytes accessed | tf_op | source)
XLA Modules:
  0.0 208.1 jit_solution(11357324409301731917)
XLA Ops:
  7.2 1.2 multiply_convert_fusion.1
  8.4 2.6 %reshape.44 = bf16[32,32,4,22]{3,2,1,0:T(4,128)(2,1)S(1)} reshape(bf16[32,2816]{1,0:T(8,128)(2,1)S(1)} %get-tuple-element.10) | data formatting | bytes 360448 | tf_op jit(solution)/shard_map/reshape | solution.py:65
  11.0 1.8 copy.22
  12.8 2.6 %reshape.45 = bf16[32,32,4,22]{3,2,1,0:T(4,128)(2,1)S(1)} reshape(bf16[32,2816]{1,0:T(8,128)(2,1)S(1)} %get-tuple-element.11) | data formatting | bytes 360448 | tf_op jit(solution)/shard_map/reshape | solution.py:65
  15.4 1.8 copy.23
  18.2 10.9 %all_to_all.27 = bf16[4,2,22528]{2,1,0:T(2,128)(2,1)S(1)} all-to-all(bf16[4,2,22528]{2,1,0:T(2,128)(2,1)S(1)} %reshape.54), channel_id=1, replica_groups=mesh['fs_0'=16,'fs_1'=4,'fs_2'=2,'tp'=4] {'tp'}, dimensions={0} | all-to-all | bytes 720896 | tf_op jit(solution)/shard_map/all_to_all | solution.py:18
  31.7 1.7 copy.26
  33.4 1.5 reshape.56
  35.0 46.7 %all_to_all.28 = bf16[128,2,704]{2,1,0:T(2,128)(2,1)S(1)} all-to-all(bf16[128,2,704]{2,1,0:T(2,128)(2,1)S(1)} %reshape.56), channel_id=1, replica_groups=mesh['fs_0'=16,'fs_1'=4,'fs_2'=2,'tp'=4] {'fs_0','fs_1','fs_2'}, dimensions={0} | all-to-all | bytes 720896 | tf_op jit(solution)/shard_map/all_to_all | solution.py:18
  81.7 1.7 reshape.57
  84.6 0.8 maximum_bitcast_fusion
  85.4 1.0 convert_element_type.27
  86.8 10.7 %all_gather.7 = bf16[88,4096]{1,0:T(8,128)(2,1)S(1)} all-gather(bf16[88,1024]{1,0:T(8,128)(2,1)S(1)} %convert_element_type.27), channel_id=1, replica_groups=mesh['fs_0'=16,'fs_1'=4,'fs_2'=2,'tp'=4] {'tp'}, dimensions={1}, use_global_device_ids=true | all-gather | bytes 901120 | tf_op jit(solution)/shard_map/all_gather | solution.py:83
  97.5 14.8 %all-gather.3.cloned.1.call-done = bf16[4,22,8192]{2,1,0:T(8,128)(2,1)} async-done(((bf16[1,22,8192]{2,1,0:T(8,128)(2,1)}), bf16[4,22,8192]{2,1,0:T(8,128)(2,1)}) %all-gather.3.cloned.1.call-update) | async-done | bytes 1441808 | tf_op jit(solution)/shard_map/all_gather | solution.py:28
  112.3 3.0 %reshape.53 = bf16[88,8192]{1,0:T(8,128)(2,1)} reshape(bf16[4,22,8192]{2,1,0:T(8,128)(2,1)} %all-gather.3.cloned.1.call-done) | data formatting | bytes 2883584
  115.3 1.4 fusion.14
  116.8 0.8 copy-done.2
  118.3 3.2 %convolution_convert_fusion = bf16[192,4096]{1,0:T(8,128)(2,1)} fusion(bf16[88,4096]{1,0:T(8,128)(2,1)S(1)} %all_gather.7, bf16[4096,88]{0,1:T(8,128)(2,1)S(1)} %get-tuple-element.17, bf16[192,4096]{1,0:T(8,128)(2,1)S(1)} %copy-done, f32[192]{0:T(256)S(1)} %add_rsqrt_fusion, f32[192,88]{0,1:T(8,128)S(1)} %fusion.5), kind=kOutput, calls=%fused_computation | convolution fusion | flops 280071168 | bytes 4655872 | tf_op jit(solution)/shard_map/dot_general | solution.py:92
  121.5 3.1 %copy.28 = bf16[192,4096]{0,1:T(8,128)(2,1)S(1)} copy(bf16[192,4096]{1,0:T(8,128)(2,1)} %convolution_convert_fusion) | data formatting | bytes 3145728 | tf_op jit(solution)/shard_map/convert_element_type | solution.py:94
  124.9 5.9 %all_to_all.29 = bf16[2,64,192,32]{2,3,1,0:T(8,128)(2,1)S(1)} all-to-all(bf16[2,64,192,32]{2,3,1,0:T(8,128)(2,1)S(1)} %copy.29), channel_id=1, replica_groups=mesh['fs_0'=16,'fs_1'=4,'fs_2'=2,'tp'=4] {'fs_2'}, dimensions={0} | all-to-all | bytes 3145728 | tf_op jit(solution)/shard_map/all_to_all | solution.py:39
  130.8 1.8 reduce_sum.34
  132.6 67.0 %all_to_all.30 = bf16[64,192,32]{1,2,0:T(8,128)(2,1)S(1)} all-to-all(bf16[64,192,32]{1,2,0:T(8,128)(2,1)} %reduce_sum.34), channel_id=1, replica_groups=mesh['fs_0'=16,'fs_1'=4,'fs_2'=2,'tp'=4] {'fs_0','fs_1'}, dimensions={0} | all-to-all | bytes 1572864 | tf_op jit(solution)/shard_map/all_to_all | solution.py:47
  199.6 0.8 reduce_sum.35
  200.4 0.9 copy.36
  (23 shorter events, 6.1 us)
Async XLA Ops:
  7.2 105.2 %all-gather.3.cloned.1.call-start = ((), (), s32[]{:S(2)}) async-start(), calls=%async_computation.4 | async-start | bytes 1966080 | tf_op jit(solution)/shard_map/all_gather | solution.py:28
  84.2 2.2 %copy-start = (bf16[192,4096]{1,0:T(8,128)(2,1)S(1)}, bf16[192,4096]{1,0:T(8,128)(2,1)}, u32[]{:S(2)}) copy-start(bf16[192,4096]{1,0:T(8,128)(2,1)} %param.5) | copy-start | bytes 4718596
  116.7 0.9 copy-start.2
  116.8 4.8 %copy-start.1 = (bf16[4096,88]{0,1:T(8,128)(2,1)}, bf16[4096,88]{0,1:T(8,128)(2,1)S(1)}, u32[]{:S(2)}) copy-start(bf16[4096,88]{0,1:T(8,128)(2,1)S(1)} %get-tuple-element.17) | copy-start | bytes 2162692
Sparse Core Ops, SparseCore 0:
  85.5 26.7 all-gather.2
where the time goes:
time: 211 us; the launch traced here: 208 us
  blocking collectives  141 us (67%)
  local copies, waits for them, and re-layouts  27.5 us (13%)
  waiting for transfers between devices  14.8 us (7%)
  between operations  14.2 us (7%)
  other arithmetic  6.46 us (3%)
  matrix products  3.93 us (2%)
    all_to_all x1, blocking collectives, sum_by_axis(): lax.all_to_all(own.astype(jnp.bfloat16), far, 0, 0, tiled=True)  67 us
    all_to_all x2, blocking collectives, in_one_piece(): lax.all_to_all(both, axis, split_axis=split_dim, concat_axis=concat_dim,...  57.6 us
    all_gather x1, waiting for transfers between devices, in_one_piece_2(): filled = lax.all_gather(both, axis, axis=dim, tiled=True)  14.8 us
    all_gather x1, blocking collectives, per_device(): lax.all_gather(down_local, 'tp', axis=1, tiled=True)  10.7 us
    unnamed x14, local copies, waits for them, and re-layouts  9.71 us
    reshape x4, local copies, waits for them, and re-layouts, arrange(): return matrix.reshape(rows_local, block_count, tp_count, piece_cols)  8.79 us
    all_to_all x1, blocking collectives, sent_and_summed(): parts = lax.all_to_all(in_blocks(array, dim, count), axis, 0, 0, tiled=True)  5.89 us
  transfers between devices with their start and end apart: 1, of which 1 were waited for; matrix products, arithmetic and copies ran while one was open for 1% of the time, Pallas kernels for 0%

commit v1 on v0

v1 whole, which is shorter than its diff:
```python
import jax
import jax.numpy as jnp
from jax import lax
from jax.experimental import pallas as pl
from jax.experimental.pallas import tpu as pltpu
from jax.sharding import Mesh
from jax.sharding import PartitionSpec as P

MESH = pl.DeviceIdType.MESH
BF = jnp.bfloat16
F32 = jnp.float32

NZ, NX, NC, NY = 16, 4, 2, 4
D, OWN, TOK, TPAD = 4096, 88, 192, 256
GROUP = 704


def lane_blocks_swapped(tiles):
    lane = lax.broadcasted_iota(jnp.int32, tiles[0].shape, 1) // 32
    outs = []
    for k in range(4):
        acc = None
        for t in range(4):
            shift = (32 * (t - k)) % 128
            moved = tiles[t] if shift == 0 else pltpu.roll(tiles[t], shift, 1)
            acc = moved if acc is None else jnp.where(lane == t, moved, acc)
        outs.append(acc)
    return outs


def kernel(
    tok, gain, gate, up, down, g_out, u_out, d_out, m_out,
    tok_v, gain_v, gu_v, down_v, normed, s_buf, ra, sb, rb, w, dn, db, d2, h, sr, rr, m_v,
    in_sem, out_sem,
    a_send, a_recv, b_send, b_recv, c_send, c_recv, d_send, d_recv, e_send, e_recv, h_send, h_recv, r_send, r_recv,
):
    z, x, c, y = (lax.axis_index(n) for n in ("z", "x", "c", "y"))
    xc = x * 2 + c
    barrier = pltpu.get_barrier_semaphore()
    here = xc * 4 + y

    def greet_plane(n, _):
        other = lax.rem(here + n, 32)
        pl.semaphore_signal(
            barrier, inc=1, device_id=(z, other // 8, lax.rem(other // 4, 2), lax.rem(other, 4)), device_id_type=MESH
        )
        return 0

    def greet_line(n, _):
        pl.semaphore_signal(barrier, inc=1, device_id=(lax.rem(z + n, NZ), x, c, y), device_id_type=MESH)
        return 0

    lax.fori_loop(1, NZ, greet_line, 0)
    lax.fori_loop(1, 32, greet_plane, 0)

    loads = [
        pltpu.make_async_copy(gate, gu_v.at[0], in_sem.at[0]),
        pltpu.make_async_copy(up, gu_v.at[1], in_sem.at[1]),
        pltpu.make_async_copy(gain, gain_v, in_sem.at[2]),
        pltpu.make_async_copy(down, down_v, in_sem.at[3]),
        pltpu.make_async_copy(tok, tok_v, in_sem.at[4]),
    ]
    for cp in loads:
        cp.start()
    loads[2].wait()
    gains = jnp.concatenate([gain_v[...]] * 4, axis=1)
    for g in range(2):
        loads[g].wait()
        stacked = jnp.concatenate([gu_v[g, :, GROUP * q : GROUP * (q + 1)] for q in range(4)], axis=0)
        turned = (jnp.transpose(stacked) * gains).astype(BF)
        for k in range(8):
            s_buf[g, k] = turned[OWN * k : OWN * (k + 1)]
    loads[3].wait()
    down_bf = down_v[...].astype(BF)
    dn[:, pl.ds(pl.multiple_of(1024 * y, 1024), 1024)] = down_bf

    pl.semaphore_wait(barrier, 46)

    half = x // 2
    sub = lax.rem(x, 2) * 2 + c

    def a_copy(n):
        to_x, to_y = lax.rem(x + n // 4, NX), lax.rem(y + n, NY)
        return pltpu.make_async_remote_copy(
            src_ref=s_buf.at[lax.rem(to_y, 2), to_x * 2 + to_y // 2],
            dst_ref=ra.at[y, sub],
            send_sem=a_send.at[n],
            recv_sem=a_recv.at[y, sub],
            device_id=(z, to_x, half, to_y),
            device_id_type=MESH,
        )

    def a_start(n, _):
        a_copy(n).start()
        return 0

    @pl.when(half != c)
    def _():
        a_copy(0).start()

    @pl.when(half == c)
    def _():
        ra[y, sub] = s_buf[lax.rem(y, 2), x * 2 + y // 2]

    lax.fori_loop(1, 16, a_start, 0)

    def d_copy(n):
        at = dn.at[:, pl.ds(pl.multiple_of(1024 * y, 1024), 1024)]
        return pltpu.make_async_remote_copy(
            src_ref=at, dst_ref=at, send_sem=d_send.at[n], recv_sem=d_recv.at[y],
            device_id=(z, x, c, lax.rem(y + n, NY)), device_id_type=MESH,
        )

    for n in (1, 3, 2):
        d_copy(n).start()

    loads[4].wait()

    def norm_rows(n, _):
        rows = pl.ds(pl.multiple_of(n * 16, 16), 16)
        t = tok_v[rows, :].astype(F32)
        normed[rows, :] = (t * lax.rsqrt(jnp.mean(t * t, axis=-1, keepdims=True) + 1e-06)).astype(BF)
        return 0

    lax.fori_loop(0, TOK // 16, norm_rows, 0)
    normed[TOK:, :] = jnp.zeros((TPAD - TOK, D), BF)

    def a_arrived(ys, s):
        @pl.when(jnp.logical_or(half != c, jnp.logical_or(ys != y, s != sub)))
        def _():
            pltpu.make_async_remote_copy(
                src_ref=ra.at[ys, s], dst_ref=ra.at[ys, s], send_sem=a_send.at[0], recv_sem=a_recv.at[ys, s],
                device_id=(z, x, 1 - c, y), device_id_type=MESH,
            ).wait_recv()

    def regroup(ys, _):
        for s in range(4):
            a_arrived(ys, s)
        outs = lane_blocks_swapped([ra[ys, s].astype(F32) for s in range(4)])
        for q in range(4):
            sb[ys * 4 + q] = outs[q].astype(BF)
        return 0

    lax.fori_loop(0, NY, regroup, 0)

    def near_first(i):
        return jnp.where(lax.rem(i, 2) == 1, (i + 1) // 2, NZ - i // 2)

    def b_copy(i):
        to_z = lax.rem(z + near_first(i), NZ)
        return pltpu.make_async_remote_copy(
            src_ref=sb.at[to_z], dst_ref=rb.at[z], send_sem=b_send.at[i], recv_sem=b_recv.at[z],
            device_id=(to_z, x, c, y), device_id_type=MESH,
        )

    def b_start(i, _):
        b_copy(i).start()
        return 0

    lax.fori_loop(1, NZ, b_start, 0)
    rb[z] = sb[z]

    own_c, own_g = y // 2, lax.rem(y, 2)

    def w_lanes(zs):
        return pl.ds(pl.multiple_of(256 * zs + 128 * c, 128), 128)

    def c_copy(zs, n):
        return pltpu.make_async_remote_copy(
            src_ref=rb.at[zs], dst_ref=w.at[own_g, :, w_lanes(zs)], send_sem=c_send.at[n], recv_sem=c_recv.at[own_g, c],
            device_id=(z, x, own_c, lax.rem(y + n, NY)), device_id_type=MESH,
        )

    def c_spread(zs):
        for n in (1, 3, 2):
            c_copy(zs, n).start()

        @pl.when(own_c != c)
        def _():
            c_copy(zs, 0).start()

        @pl.when(own_c == c)
        def _():
            w[own_g, :, w_lanes(zs)] = rb[zs]

    c_spread(z)

    def c_step(i, _):
        zs = lax.rem(z + NZ - near_first(i), NZ)
        pltpu.make_async_remote_copy(
            src_ref=rb.at[zs], dst_ref=rb.at[zs], send_sem=b_send.at[0], recv_sem=b_recv.at[zs],
            device_id=(lax.rem(z + 1, NZ), x, c, y), device_id_type=MESH,
        ).wait_recv()
        c_spread(zs)
        return 0

    lax.fori_loop(1, 8, c_step, 0)

    for n in (1, 2, 3):
        ys = lax.rem(y + NY - n, NY)
        at = dn.at[:, pl.ds(pl.multiple_of(1024 * ys, 1024), 1024)]
        pltpu.make_async_remote_copy(
            src_ref=at, dst_ref=at, send_sem=d_send.at[0], recv_sem=d_recv.at[ys],
            device_id=(z, x, 1 - c, y), device_id_type=MESH,
        ).wait_recv()
    d_store = pltpu.make_async_copy(dn, d_out, out_sem.at[2])
    d_store.start()

    def by_column(n, _):
        ys, hi = n // 2, lax.rem(n, 2)
        tiles = [
            dn[:, pl.ds(pl.multiple_of(1024 * ys + 256 * q + 128 * hi, 128), 128)].astype(F32) for q in range(4)
        ]
        outs = lane_blocks_swapped(tiles)
        for k in range(4):
            db[hi * 4 + k, :, pl.ds(pl.multiple_of(128 * ys, 128), 128)] = outs[k].astype(BF)
        return 0

    lax.fori_loop(0, 8, by_column, 0)

    def e_copy(n):
        to = lax.rem(xc + n, 8)
        return pltpu.make_async_remote_copy(
            src_ref=db.at[to], dst_ref=d2.at[xc], send_sem=e_send.at[n], recv_sem=e_recv.at[xc],
            device_id=(z, to // 2, lax.rem(to, 2), y), device_id_type=MESH,
        )

    def e_start(n, _):
        e_copy(n).start()
        return 0

    lax.fori_loop(1, 8, e_start, 0)
    d2[xc] = db[xc]

    lax.fori_loop(8, NZ, c_step, 0)

    stores = [d_store]
    for g in range(2):
        for k in range(2):
            @pl.when(jnp.logical_or(y != 2 * c + g, c != k))
            def _():
                pltpu.make_async_remote_copy(
                    src_ref=rb, dst_ref=rb, send_sem=c_send.at[0], recv_sem=c_recv.at[g, k],
                    device_id=(z, x, 1 - c, y), device_id_type=MESH,
                ).wait_recv()
        stores.append(pltpu.make_async_copy(w.at[g], (g_out, u_out)[g], out_sem.at[g]))
        stores[-1].start()

    acts = [
        lax.dot_general(w[g], normed[...], (((1,), (1,)), ((), ())), preferred_element_type=F32) for g in range(2)
    ]
    h[xc] = (acts[0] / (1.0 + jnp.exp(-acts[0])) * acts[1]).astype(BF)

    def h_copy(n):
        to = lax.rem(xc + n, 8)
        return pltpu.make_async_remote_copy(
            src_ref=h.at[xc], dst_ref=h.at[xc], send_sem=h_send.at[n], recv_sem=h_recv.at[xc],
            device_id=(z, to // 2, lax.rem(to, 2), y), device_id_type=MESH,
        )

    def h_start(n, _):
        h_copy(n).start()
        return 0

    lax.fori_loop(1, 8, h_start, 0)

    def plane_arrived(n, _):
        fr = lax.rem(xc + 8 - n, 8)
        pltpu.make_async_remote_copy(
            src_ref=d2.at[fr], dst_ref=d2.at[fr], send_sem=e_send.at[0], recv_sem=e_recv.at[fr],
            device_id=(z, x, 1 - c, y), device_id_type=MESH,
        ).wait_recv()
        pltpu.make_async_remote_copy(
            src_ref=h.at[fr], dst_ref=h.at[fr], send_sem=h_send.at[0], recv_sem=h_recv.at[fr],
            device_id=(z, x, 1 - c, y), device_id_type=MESH,
        ).wait_recv()
        return 0

    lax.fori_loop(1, 8, plane_arrived, 0)
    part = lax.dot_general(
        d2[...].reshape(8 * OWN, 512), h[...].reshape(8 * OWN, TPAD), (((0,), (0,)), ((), ())),
        preferred_element_type=F32,
    )
    lane = lax.broadcasted_iota(jnp.int32, (16, 128), 1)
    for q in range(NZ):
        block = part[32 * q : 32 * (q + 1)]
        tail = block[:, 128:]
        sr[q, :32] = block[:, :128].astype(BF)
        sr[q, 32:] = jnp.where(lane < 64, tail[:16], pltpu.roll(tail[16:], 64, 1)).astype(BF)

    def r_copy(i):
        to_z = lax.rem(z + near_first(i), NZ)
        return pltpu.make_async_remote_copy(
            src_ref=sr.at[to_z], dst_ref=rr.at[z], send_sem=r_send.at[i], recv_sem=r_recv.at[z],
            device_id=(to_z, x, c, y), device_id_type=MESH,
        )

    def r_start(i, _):
        r_copy(NZ - i).start()
        return 0

    lax.fori_loop(1, NZ, r_start, 0)

    def r_arrived(i, total):
        zs = lax.rem(z + NZ - near_first(i), NZ)
        pltpu.make_async_remote_copy(
            src_ref=rr.at[zs], dst_ref=rr.at[zs], send_sem=r_send.at[0], recv_sem=r_recv.at[zs],
            device_id=(lax.rem(z + 1, NZ), x, c, y), device_id_type=MESH,
        ).wait_recv()
        return total + rr[zs].astype(F32)

    total = lax.fori_loop(1, NZ, r_arrived, sr[z].astype(F32))
    m_v[:, :128] = total[:32].astype(BF)
    m_v[:16, 128:] = total[32:, :64].astype(BF)
    m_v[16:, 128:] = pltpu.roll(total[32:], 64, 1)[:, :64].astype(BF)
    m_store = pltpu.make_async_copy(m_v, m_out, out_sem.at[3])
    m_store.start()
    stores.append(m_store)

    @pl.when(half != c)
    def _():
        a_copy(0).wait_send()

    def a_sent(n, _):
        a_copy(n).wait_send()
        return 0

    lax.fori_loop(1, 16, a_sent, 0)

    def line_sent(i, _):
        b_copy(i).wait_send()
        r_copy(i).wait_send()
        return 0

    lax.fori_loop(1, NZ, line_sent, 0)

    def plane_sent(n, _):
        e_copy(n).wait_send()
        h_copy(n).wait_send()
        return 0

    lax.fori_loop(1, 8, plane_sent, 0)

    def c_sent(n):
        pltpu.make_async_remote_copy(
            src_ref=rb, dst_ref=rb, send_sem=c_send.at[n], recv_sem=c_recv.at[0, 0],
            device_id=(z, x, 1 - c, y), device_id_type=MESH,
        ).wait_send()

    for n in (1, 2, 3):
        d_copy(n).wait_send()
        c_sent(n)

    @pl.when(own_c != c)
    def _():
        c_sent(0)

    for cp in stores:
        cp.wait()


def per_device(tokens, norm_gain, gate_trained, up_trained, down_trained):
    dma = pltpu.SemaphoreType.DMA
    g_t, u_t, d_o, m_t = pl.pallas_call(
        kernel,
        out_shape=(
            jax.ShapeDtypeStruct((OWN, D), BF),
            jax.ShapeDtypeStruct((OWN, D), BF),
            jax.ShapeDtypeStruct((OWN, D), BF),
            jax.ShapeDtypeStruct((32, TOK), BF),
        ),
        in_specs=[pl.BlockSpec(memory_space=pltpu.HBM)] * 5,
        out_specs=(pl.BlockSpec(memory_space=pltpu.HBM),) * 4,
        scratch_shapes=[
            pltpu.VMEM((TOK, D), BF),
            pltpu.VMEM((1, 32), F32),
            pltpu.VMEM((2, 32, 4 * GROUP), F32),
            pltpu.VMEM((OWN, 1024), F32),
            pltpu.VMEM((TPAD, D), BF),
            pltpu.VMEM((2, 8, OWN, 128), BF),
            pltpu.VMEM((NY, 4, OWN, 128), BF),
            pltpu.VMEM((NZ, OWN, 128), BF),
            pltpu.VMEM((NZ, OWN, 128), BF),
            pltpu.VMEM((2, OWN, D), BF),
            pltpu.VMEM((OWN, D), BF),
            pltpu.VMEM((8, OWN, 512), BF),
            pltpu.VMEM((8, OWN, 512), BF),
            pltpu.VMEM((8, OWN, TPAD), BF),
            pltpu.VMEM((NZ, 48, 128), BF),
            pltpu.VMEM((NZ, 48, 128), BF),
            pltpu.VMEM((32, TOK), BF),
            dma((5,)),
            dma((4,)),
            dma((16,)),
            dma((NY, 4)),
            dma((NZ,)),
            dma((NZ,)),
            dma((NY,)),
            dma((2, 2)),
            dma((NY,)),
            dma((NY,)),
            dma((8,)),
            dma((8,)),
            dma((8,)),
            dma((8,)),
            dma((NZ,)),
            dma((NZ,)),
        ],
        compiler_params=pltpu.CompilerParams(
            collective_id=0, has_side_effects=True, vmem_limit_bytes=48 * 1024 * 1024
        ),
        name="handoff",
    )(tokens, norm_gain.reshape(1, 32), gate_trained, up_trained, down_trained)
    return jnp.transpose(g_t), jnp.transpose(u_t), d_o, jnp.transpose(m_t)


def solution(mesh):
    split = Mesh(mesh.devices.reshape(NZ, NX, NC, NY), ("z", "x", "c", "y"))
    fs = ("z", "x", "c")
    in_specs = (P("y", None), P(fs), P(fs, "y"), P(fs, "y"), P(fs, "y"))
    out_specs = (P(None, fs), P(None, fs), P(fs, None), P("y", fs))
    return jax.shard_map(per_device, mesh=split, in_specs=in_specs, out_specs=out_specs, check_vma=False)
```

time: 211 us -> 77.9 us (0.37); the launches traced: 208 us -> 77.6 us
  blocking collectives: 141 us -> 0 us
  Pallas kernels: 0 us -> 68.8 us
  local copies, waits for them, and re-layouts: 27.5 us -> 8.19 us
  waiting for transfers between devices: 14.8 us -> 0 us
  between operations: 14.2 us -> 0.65 us
  other arithmetic: 6.46 us -> 0 us
  matrix products: 3.93 us -> 0 us
    all_to_all x4 -> x0, blocking collectives: 130 us -> none  [the longest x1 67 us: sum_by_axis(): lax.all_to_all(own.astype(jnp.bfloat16), far, 0, 0, tiled=True)]
    pallas_call x0 -> x1, Pallas kernels: none -> 68.8 us  [per_device(): pl.pallas_call(kernel, out_shape=(jax.ShapeDtypeStruct((OWN, D), BF), jax...]
    all_gather x1 -> x0, waiting for transfers between devices: 14.8 us -> none  [in_one_piece_2(): filled = lax.all_gather(both, axis, axis=dim, tiled=True)]
    all_gather x1 -> x0, blocking collectives: 10.7 us -> none  [per_device(): lax.all_gather(down_local, 'tp', axis=1, tiled=True)]
    reshape x6 -> x0, local copies, waits for them, and re-layouts: 9.5 us -> none  [the longest x4 8.79 us: arrange(): return matrix.reshape(rows_local, block_count, tp_count, piece_cols)]
    dot_general x2 -> x0, matrix products: 3.93 us -> none  [the longest x1 3.21 us: per_device(): jnp.dot(hidden, down_sampler, preferred_element_type=jnp.float32)]
    convert_element_type x1 -> x0, local copies, waits for them, and re-layouts: 3.15 us -> none  [per_device(): partial_terms.astype(jnp.bfloat16)]
    reduce_sum x3 -> x0, other arithmetic: 3.01 us -> none  [the longest x1 1.8 us: sent_and_summed(): return jnp.sum(parts.astype(jnp.float32), axis=0)]
  transfers between devices with their start and end apart: 1 -> 0, of which waited for: 1 -> 0; matrix products, arithmetic and copies ran while one was open for 1% -> 0% of each run, Pallas kernels for 0% -> 0%
where the time goes in v1:
time: 77.9 us; the launch traced here: 77.6 us
  Pallas kernels  68.8 us (88%)
  local copies, waits for them, and re-layouts  8.19 us (11%)
    pallas_call x1, Pallas kernels, per_device(): pl.pallas_call(kernel, out_shape=(jax.ShapeDtypeStruct((OWN, D), BF), jax...  68.8 us
    unnamed x14, local copies, waits for them, and re-layouts  8.19 us

profile of v1, /device:TPU:1, one launch (start us, length us, event | category | flops | bytes accessed | tf_op | source)
XLA Modules:
  0.0 77.6 jit_solution(13760191718301356561)
XLA Ops:
  0.6 0.0 copy-start
  0.6 1.4 %copy-done = bf16[192,4096]{1,0:T(8,128)(2,1)S(1)} copy-done((bf16[192,4096]{1,0:T(8,128)(2,1)S(1)}, bf16[192,4096]{1,0:T(8,128)(2,1)}, u32[]{:S(2)}) %copy-start) | copy-done | bytes 1572888
  2.0 0.0 copy-start.1
  2.0 1.0 %copy-done.1 = f32[32,2816]{1,0:T(8,128)S(1)} copy-done((f32[32,2816]{1,0:T(8,128)S(1)}, f32[32,2816]{1,0:T(8,128)}, u32[]{:S(2)}) %copy-start.1) | copy-done | bytes 360472
  3.0 0.0 copy-start.2
  3.0 1.0 %copy-done.2 = f32[32,2816]{1,0:T(8,128)S(1)} copy-done((f32[32,2816]{1,0:T(8,128)S(1)}, f32[32,2816]{1,0:T(8,128)}, u32[]{:S(2)}) %copy-start.2) | copy-done | bytes 360472
  4.0 0.0 copy-start.3
  4.0 1.0 %copy-done.3 = f32[88,1024]{1,0:T(8,128)S(1)} copy-done((f32[88,1024]{1,0:T(8,128)S(1)}, f32[88,1024]{1,0:T(8,128)}, u32[]{:S(2)}) %copy-start.3) | copy-done | bytes 360472
  5.0 0.0 copy-start.4
  5.0 0.7 copy-done.4
  5.7 68.8 %handoff.1 = (bf16[88,4096]{1,0:T(8,128)(2,1)S(1)}, bf16[88,4096]{1,0:T(8,128)(2,1)S(1)}, bf16[88,4096]{1,0:T(8,128)(2,1)S(1)}, bf16[32,192]{1,0:T(8,128)(2,1)S(1)}) custom-call(bf16[192,4096]{1,0:T(8,128)(2,1)S(1)} %copy-done, f32[1,32]{1,0:T(1,128)S(1)} %bitcast.7, f32[32,2816]{1,0:T(8,128)S(1)} %copy-done.1, f32[32,2816]{1,0:T(8,128)S(1)} %copy-done.2, ...), custom_call_target="tpu_custom_call" | custom-call | tf_op jit(solution)/shard_map/handoff/pallas_call | solution.py:364
  74.4 0.9 %copy.13 = bf16[4096,88]{0,1:T(8,128)(2,1)} copy(bf16[4096,88]{0,1:T(8,128)(2,1)S(1)} %bitcast.5) | data formatting | bytes 1441792
  75.3 0.9 %copy.14 = bf16[4096,88]{0,1:T(8,128)(2,1)} copy(bf16[4096,88]{0,1:T(8,128)(2,1)S(1)} %bitcast.4) | data formatting | bytes 1441792
  76.1 0.9 %copy.15 = bf16[88,4096]{1,0:T(8,128)(2,1)} copy(bf16[88,4096]{1,0:T(8,128)(2,1)S(1)} %get-tuple-element.18) | data formatting | bytes 1441792
  77.0 0.6 copy.16
Async XLA Ops:
  0.6 1.4 %copy-start = (bf16[192,4096]{1,0:T(8,128)(2,1)S(1)}, bf16[192,4096]{1,0:T(8,128)(2,1)}, u32[]{:S(2)}) copy-start(bf16[192,4096]{1,0:T(8,128)(2,1)} %tok.1) | copy-start | bytes 4718596
  2.0 1.0 %copy-start.1 = (f32[32,2816]{1,0:T(8,128)S(1)}, f32[32,2816]{1,0:T(8,128)}, u32[]{:S(2)}) copy-start(f32[32,2816]{1,0:T(8,128)} %gate.1) | copy-start | bytes 1081348
  3.0 1.0 %copy-start.2 = (f32[32,2816]{1,0:T(8,128)S(1)}, f32[32,2816]{1,0:T(8,128)}, u32[]{:S(2)}) copy-start(f32[32,2816]{1,0:T(8,128)} %up.1) | copy-start | bytes 1081348
  4.0 1.0 %copy-start.3 = (f32[88,1024]{1,0:T(8,128)S(1)}, f32[88,1024]{1,0:T(8,128)}, u32[]{:S(2)}) copy-start(f32[88,1024]{1,0:T(8,128)} %down.1) | copy-start | bytes 1081348
  5.0 0.7 copy-start.4

commit v2 on v1

--- a/solution.py
+++ b/solution.py
@@ -6,6 +6,7 @@
 from jax.sharding import Mesh
 from jax.sharding import PartitionSpec as P
 
+LIMIT = 62000000
 MESH = pl.DeviceIdType.MESH
 BF = jnp.bfloat16
 F32 = jnp.float32
@@ -36,23 +37,6 @@
 ):
     z, x, c, y = (lax.axis_index(n) for n in ("z", "x", "c", "y"))
     xc = x * 2 + c
-    barrier = pltpu.get_barrier_semaphore()
-    here = xc * 4 + y
-
-    def greet_plane(n, _):
-        other = lax.rem(here + n, 32)
-        pl.semaphore_signal(
-            barrier, inc=1, device_id=(z, other // 8, lax.rem(other // 4, 2), lax.rem(other, 4)), device_id_type=MESH
-        )
-        return 0
-
-    def greet_line(n, _):
-        pl.semaphore_signal(barrier, inc=1, device_id=(lax.rem(z + n, NZ), x, c, y), device_id_type=MESH)
-        return 0
-
-    lax.fori_loop(1, NZ, greet_line, 0)
-    lax.fori_loop(1, 32, greet_plane, 0)
-
     loads = [
         pltpu.make_async_copy(gate, gu_v.at[0], in_sem.at[0]),
         pltpu.make_async_copy(up, gu_v.at[1], in_sem.at[1]),
@@ -62,6 +46,23 @@
     ]
     for cp in loads:
         cp.start()
+    barrier = pltpu.get_barrier_semaphore()
+    here = xc * 4 + y
+
+    def greet_plane(n, _):
+        other = lax.rem(here + n, 32)
+        pl.semaphore_signal(
+            barrier, inc=1, device_id=(z, other // 8, lax.rem(other // 4, 2), lax.rem(other, 4)), device_id_type=MESH
+        )
+        return 0
+
+    def greet_line(n, _):
+        pl.semaphore_signal(barrier, inc=1, device_id=(lax.rem(z + n, NZ), x, c, y), device_id_type=MESH)
+        return 0
+
+    lax.fori_loop(1, NZ, greet_line, 0)
+    lax.fori_loop(1, 32, greet_plane, 0)
+
     loads[2].wait()
     gains = jnp.concatenate([gain_v[...]] * 4, axis=1)
     for g in range(2):
@@ -359,18 +360,29 @@
         cp.wait()
 
 
+def hand_over(g_t, u_t, d_o, m_t, g_out, u_out, d_out, m_out, sem):
+    copies = [
+        pltpu.make_async_copy(a, b, sem.at[n])
+        for n, (a, b) in enumerate(((g_t, g_out), (u_t, u_out), (d_o, d_out), (m_t, m_out)))
+    ]
+    for cp in copies:
+        cp.start()
+    for cp in copies:
+        cp.wait()
+
+
 def per_device(tokens, norm_gain, gate_trained, up_trained, down_trained):
     dma = pltpu.SemaphoreType.DMA
     g_t, u_t, d_o, m_t = pl.pallas_call(
         kernel,
         out_shape=(
-            jax.ShapeDtypeStruct((OWN, D), BF),
-            jax.ShapeDtypeStruct((OWN, D), BF),
-            jax.ShapeDtypeStruct((OWN, D), BF),
-            jax.ShapeDtypeStruct((32, TOK), BF),
+            pltpu.VMEM((OWN, D), BF),
+            pltpu.VMEM((OWN, D), BF),
+            pltpu.VMEM((OWN, D), BF),
+            pltpu.VMEM((32, TOK), BF),
         ),
         in_specs=[pl.BlockSpec(memory_space=pltpu.HBM)] * 5,
-        out_specs=(pl.BlockSpec(memory_space=pltpu.HBM),) * 4,
+        out_specs=(pl.BlockSpec(memory_space=pltpu.VMEM),) * 4,
         scratch_shapes=[
             pltpu.VMEM((TOK, D), BF),
             pltpu.VMEM((1, 32), F32),
@@ -407,10 +419,19 @@
             dma((NZ,)),
         ],
         compiler_params=pltpu.CompilerParams(
-            collective_id=0, has_side_effects=True, vmem_limit_bytes=48 * 1024 * 1024
+            collective_id=0, has_side_effects=True, vmem_limit_bytes=LIMIT
         ),
         name="handoff",
     )(tokens, norm_gain.reshape(1, 32), gate_trained, up_trained, down_trained)
+    g_t, u_t, d_o, m_t = pl.pallas_call(
+        hand_over,
+        out_shape=tuple(jax.ShapeDtypeStruct(a.shape, a.dtype) for a in (g_t, u_t, d_o, m_t)),
+        in_specs=[pl.BlockSpec(memory_space=pltpu.VMEM)] * 4,
+        out_specs=(pl.BlockSpec(memory_space=pltpu.HBM),) * 4,
+        scratch_shapes=[pltpu.SemaphoreType.DMA((4,))],
+        compiler_params=pltpu.CompilerParams(vmem_limit_bytes=8 * 1024 * 1024),
+        name="hand_over",
+    )(g_t, u_t, d_o, m_t)
     return jnp.transpose(g_t), jnp.transpose(u_t), d_o, jnp.transpose(m_t)
 
 

time: 77.9 us -> 71.3 us (0.915)
  local copies, waits for them, and re-layouts: 8.19 us -> 0 us
  Pallas kernels: 68.8 us -> 70.6 us
    unnamed x14 -> x0, local copies, waits for them, and re-layouts: 8.19 us -> none
    pallas_call x1 -> x2, Pallas kernels: 68.8 us -> 70.6 us  [the longest x1 69.2 us: per_device(): pl.pallas_call(kernel, out_shape=(pltpu.VMEM((OWN, D), BF), pltpu.VMEM((O...]
where the time goes in v2:
time: 71.3 us; the launch traced here: 71.2 us
  Pallas kernels  70.6 us (99%)
    pallas_call x1, Pallas kernels, per_device(): pl.pallas_call(kernel, out_shape=(pltpu.VMEM((OWN, D), BF), pltpu.VMEM((O...  69.2 us

profile of v2, /device:TPU:1, one launch (start us, length us, event | category | flops | bytes accessed | tf_op | source)
XLA Modules:
  0.0 71.2 jit_solution(1202829100964713035)
XLA Ops:
  0.6 69.2 %handoff.1 = (bf16[88,4096]{1,0:T(8,128)(2,1)S(1)}, bf16[88,4096]{1,0:T(8,128)(2,1)S(1)}, bf16[88,4096]{1,0:T(8,128)(2,1)S(1)}, bf16[32,192]{1,0:T(8,128)(2,1)S(1)}) custom-call(bf16[192,4096]{1,0:T(8,128)(2,1)} %tok.1, f32[1,32]{1,0:T(1,128)} %bitcast.4, f32[32,2816]{1,0:T(8,128)} %gate.1, f32[32,2816]{1,0:T(8,128)} %up.1, f32[88,1024]{1,0:T(8,128)} %down.1), custom_call_target="tpu_custom_call" | custom-call | tf_op jit(solution)/shard_map/handoff/pallas_call | solution.py:376
  69.8 1.4 %hand_over.1 = (bf16[88,4096]{1,0:T(8,128)(2,1)}, bf16[88,4096]{1,0:T(8,128)(2,1)}, bf16[88,4096]{1,0:T(8,128)(2,1)}, bf16[32,192]{1,0:T(8,128)(2,1)}) custom-call(bf16[88,4096]{1,0:T(8,128)(2,1)S(1)} %get-tuple-element.12.g_t, bf16[88,4096]{1,0:T(8,128)(2,1)S(1)} %get-tuple-element.13.u_t, bf16[88,4096]{1,0:T(8,128)(2,1)S(1)} %get-tuple-element.14.d_o, ...), custom_call_target="tpu_custom_call" | custom-call | tf_op jit(solution)/shard_map/hand_over/pallas_call | solution.py:426
